TPU v7x, 32 devices: a whole 2x2x4 slice. The times are simulated.
32 devices in a mesh: sp: 8 (over z, core), tp: 4 (over y, x).
Axes of the slice: x: 2, y: 2, z: 4, core: 2. Of those that a mesh axis runs over, the one named last changes fastest.
Arguments:
- cell_query_heads: bfloat16 [1024, 2048], P('sp', 'tp'), may hold values from -6 to 6
- cell_key_heads: bfloat16 [1024, 2048], P('sp', 'tp'), may hold values from -6 to 6
- cell_value_heads: bfloat16 [1024, 2048], P('sp', 'tp'), may hold values from -6 to 6
- output_gate_logits: bfloat16 [1024, 2048], P('sp', 'tp'), may hold values from -6 to 6
- input_gate_log: float32 [1024, 16], P('sp', 'tp'), may hold values from -7 to 310
- forget_gate_logits: float32 [1024, 16], P('sp', 'tp'), may hold values from 1 to 14
- extra_log_decay: float32 [1024, 16], P('sp', 'tp'), may hold values from -1 to 0
- documents: int32 [1024], P('sp'), may hold values from 0 to 7, never falling along the last dimension, each value on 1 to 256 neighbouring positions
- head_norm_gain: float32 [2048], P('tp'), may hold values from 0.1 to 1.9
- stream: bfloat16 [1024, 4096], P('sp', 'tp'), may hold values from -6 to 6
- output_weight: bfloat16 [2048, 4096], P(None, 'tp'), may hold values from -0.125 to 0.125
- expert_norm_gain: bfloat16 [4096], P('tp'), may hold values from 0.099609375 to 1.8984375
- expert_choice_index: int32 [1024, 2], P('sp'), may hold values from 0 to 7, all different within a row; in each aligned block of 128 rows (0 to 127, 128 to 255, ...) at most 64 rows name the same one
- routing_weight: float32 [1024, 2], P('sp'), may hold values from 0.2 to 1
- gate_weight: bfloat16 [8, 4096, 2048], P('sp', None, 'tp'), may hold values from -0.09375 to 0.09375
- up_weight: bfloat16 [8, 4096, 2048], P('sp', None, 'tp'), may hold values from -0.09375 to 0.09375
- down_weight: bfloat16 [8, 2048, 4096], P('sp', None, 'tp'), may hold values from -0.125 to 0.125
Outputs:
- output: bfloat16 [1024, 4096], P('sp', 'tp')
Inputs may be any that keep to these rules, and one draw needn't show every extreme that they name: `expert_choice_index`: in the rows of one index of sp no expert is named more than 64 times, a bound that some block reaches. `documents`: never falling; each document 1 to 256 positions, one exactly 256.
All inputs are finite; a program needn't handle non-finite values.
Results may differ from a plain program's by a relative error of at most 0.01.
Values may be sent and summed in bfloat16 or wider, within the bound.
A program may use at most 64 MiB of HBM per device.

v0:
```python
import jax
import jax.numpy as jnp
from jax import lax
from jax.sharding import PartitionSpec as P

D = 4096
HD = 128
TOPK = 2
EPSILON = 1e-06
LOW_LOG = -1e30
HIGHEST = lax.Precision.HIGHEST


def prefix_2(part, axis, combine, identity):
    place = lax.axis_index(axis)
    gathered = jax.tree.map(lambda a: lax.all_gather(a, axis), part)
    state = jax.tree.map(lambda a, e: jnp.zeros_like(a) + jnp.asarray(e, a.dtype), part, identity)

    def one(turn, state):
        return combine(
            state, jax.tree.map(lambda a: lax.dynamic_index_in_dim(a, turn, 0, False), gathered)
        )

    return lax.fori_loop(0, place, one, state)


def empty_summary(heads, width):
    return (
        jnp.zeros((heads, width, width), jnp.float32),
        jnp.zeros((heads, width), jnp.float32),
        jnp.full((heads,), LOW_LOG, jnp.float32),
        jnp.zeros((heads,), jnp.float32),
        jnp.zeros((), jnp.int32),
        jnp.full((), -1, jnp.int32),
        jnp.full((), -1, jnp.int32),
    )


def block_summary(key_f, value_f, decay_logarithm, input_gate_log, documents, first_global):
    length = documents.shape[0]
    positions = jnp.arange(length, dtype=jnp.int32)
    cumulative = jnp.cumsum(decay_logarithm, axis=0)
    total_log = cumulative[-1]
    prior_log = cumulative - decay_logarithm
    starts = jnp.concatenate([jnp.reshape(first_global, (1,)), documents[1:] != documents[:-1]])
    inside = jnp.any(starts)
    last_start = jnp.max(jnp.where(starts, positions, -1))
    base_log = jnp.sum(jnp.where((positions == last_start)[:, None], prior_log, 0.0), axis=0)
    in_last = (documents == documents[-1])[:, None]
    weight_log = total_log[None, :] - cumulative + input_gate_log
    peak_log = jnp.max(jnp.where(in_last, weight_log, LOW_LOG), axis=0)
    peak_log = jnp.where(inside, jnp.maximum(peak_log, total_log - base_log), peak_log)
    weights = jnp.where(in_last, jnp.exp(jnp.minimum(weight_log - peak_log[None, :], 0.0)), 0.0)
    matrix = jnp.einsum("lhd,lhe->hde", weights[:, :, None] * key_f, value_f, precision=HIGHEST)
    normer = jnp.sum(weights[:, :, None] * key_f, axis=0)
    return (
        matrix,
        normer,
        peak_log,
        total_log,
        inside.astype(jnp.int32),
        documents[0],
        documents[-1],
    )


def combine(early, late):
    broken = late[5] != early[6]
    carry_matrix = jnp.where(broken, 0.0, early[0])
    carry_normer = jnp.where(broken, 0.0, early[1])
    carry_peak = jnp.where(broken, 0.0, early[2])
    joined = jnp.maximum(late[3] + carry_peak, late[2])
    older = jnp.exp(late[3] + carry_peak - joined)
    newer = jnp.exp(late[2] - joined)
    resets = late[4] > 0
    matrix = jnp.where(
        resets, late[0], older[:, None, None] * carry_matrix + newer[:, None, None] * late[0]
    )
    normer = jnp.where(resets, late[1], older[:, None] * carry_normer + newer[:, None] * late[1])
    peak_log = jnp.where(resets, late[2], joined)
    flags = jnp.maximum(jnp.maximum(early[4], late[4]), broken.astype(jnp.int32))
    merged = (matrix, normer, peak_log, early[3] + late[3], flags, early[5], late[6])
    early_empty = early[6] < 0
    late_empty = late[6] < 0
    return tuple(
        (
            jnp.where(early_empty, second, jnp.where(late_empty, first_item, joint))
            for first_item, second, joint in zip(early, late, merged)
        )
    )


def block_output(query_f, key_f, value_f, decay_logarithm, input_gate_log, documents, prefix):
    prev_matrix, prev_normer, prev_peak, _, _, _, prev_last = prefix
    length = documents.shape[0]
    positions = jnp.arange(length, dtype=jnp.int32)
    cumulative = jnp.cumsum(decay_logarithm, axis=0)
    prior_log = cumulative - decay_logarithm
    before = jnp.concatenate([jnp.reshape(prev_last, (1,)), documents[:-1]])
    starts = documents != before
    last_start = lax.cummax(jnp.where(starts, positions, -1), axis=0)
    started = last_start >= 0
    picker = (positions[None, :] == last_start[:, None]).astype(jnp.float32)
    base_log = jnp.dot(picker, prior_log, precision=HIGHEST)
    carry_log = (cumulative + jnp.where(started[:, None], -base_log, prev_peak[None, :])).T
    same_doc = (documents[:, None] == documents[None, :]) & (
        positions[:, None] >= positions[None, :]
    )
    cum_heads = cumulative.T
    pair_log = cum_heads[:, :, None] - cum_heads[:, None, :] + input_gate_log.T[:, None, :]
    pair_log = jnp.where(same_doc[None], pair_log, LOW_LOG)
    peak_log = jnp.maximum(carry_log, jnp.max(pair_log, axis=-1))
    weights = jnp.exp(pair_log - peak_log[:, :, None])
    scores = jnp.einsum("lhd,shd->hls", query_f, key_f, precision=HIGHEST) * weights
    carry_scale = jnp.where(started[None, :], 0.0, jnp.exp(carry_log - peak_log))
    numer = jnp.einsum("hls,she->hle", scores, value_f, precision=HIGHEST)
    numer = numer + carry_scale[:, :, None] * jnp.einsum(
        "lhd,hde->hle", query_f, prev_matrix, precision=HIGHEST
    )
    denom = jnp.sum(scores, axis=-1) + carry_scale * jnp.einsum(
        "lhd,hd->hl", query_f, prev_normer, precision=HIGHEST
    )
    cell_vals = numer / jnp.maximum(jnp.abs(denom), jnp.exp(-peak_log))[:, :, None]
    return jnp.transpose(cell_vals, (1, 0, 2))


def finish_cell(cell_vals, output_gate_logits, head_norm_gain):
    length, heads, width = cell_vals.shape
    gated_cell = (
        jax.nn.sigmoid(output_gate_logits.astype(jnp.float32)).reshape(length, heads, width)
        * cell_vals
    )
    scaled = gated_cell * lax.rsqrt(
        jnp.mean(gated_cell * gated_cell, axis=-1, keepdims=True) + EPSILON
    )
    scaled = scaled * head_norm_gain.reshape(heads, width)
    return scaled.reshape(length, heads * width).astype(jnp.bfloat16)


def expert_work(row_block, gate_weight, up_weight, down_weight):
    gate_act = jnp.einsum(
        "sqid,qdf->sqif", row_block, gate_weight, preferred_element_type=jnp.float32
    )
    upward = jnp.einsum("sqid,qdf->sqif", row_block, up_weight, preferred_element_type=jnp.float32)
    hidden = (jax.nn.silu(gate_act) * upward).astype(jnp.bfloat16)
    result = jnp.einsum(
        "sqif,qfe->sqie",
        lax.all_gather(hidden, "tp", axis=3, tiled=True),
        down_weight,
        preferred_element_type=jnp.float32,
    )
    return result.astype(jnp.bfloat16)


def per_device(
    cell_query_heads,
    cell_key_heads,
    cell_value_heads,
    output_gate_logits,
    input_gate_log,
    forget_gate_logits,
    extra_log_decay,
    documents,
    head_norm_gain,
    stream,
    output_weight,
    expert_norm_gain,
    expert_choice_index,
    routing_weight,
    gate_weight,
    up_weight,
    down_weight,
):
    tokens = documents.shape[0]
    local_heads = input_gate_log.shape[1]
    shaped = (tokens, local_heads, HD)
    query_f = cell_query_heads.astype(jnp.float32).reshape(shaped)
    key_f = cell_key_heads.astype(jnp.float32).reshape(shaped) * HD ** (-0.5)
    value_f = cell_value_heads.astype(jnp.float32).reshape(shaped)
    decay_logarithm = jax.nn.log_sigmoid(forget_gate_logits) + extra_log_decay
    first_global = lax.axis_index("sp") == 0
    summary = block_summary(
        key_f, value_f, decay_logarithm, input_gate_log, documents, first_global
    )
    prefix = prefix_2(summary, "sp", combine, empty_summary(local_heads, HD))
    cell_vals = block_output(
        query_f, key_f, value_f, decay_logarithm, input_gate_log, documents, prefix
    )
    memory_cell_output = finish_cell(cell_vals, output_gate_logits, head_norm_gain)
    projected = jnp.dot(
        lax.all_gather(memory_cell_output, "tp", axis=1, tiled=True),
        output_weight,
        preferred_element_type=jnp.float32,
    )
    resid = (stream.astype(jnp.float32) + projected).astype(jnp.bfloat16)
    groups = lax.axis_size("sp")
    experts_all = groups * gate_weight.shape[0]
    capacity = 2 * tokens * TOPK // experts_all
    flat_ids = expert_choice_index.reshape(-1)
    onehot = (flat_ids[:, None] == jnp.arange(experts_all, dtype=jnp.int32)[None, :]).astype(
        jnp.int32
    )
    rank_in = jnp.sum((jnp.cumsum(onehot, axis=0) - onehot) * onehot, axis=1)
    slot_of = (flat_ids * capacity + rank_in).reshape(tokens, TOPK)
    slot_index = jnp.arange(experts_all * capacity, dtype=jnp.int32)
    chooser = jnp.any(slot_index[:, None, None] == slot_of[None, :, :], axis=2).astype(jnp.bfloat16)
    bucket_shape = (groups, gate_weight.shape[0], capacity)
    rows_f = resid.astype(jnp.float32)
    squares = lax.psum(jnp.sum(rows_f * rows_f, axis=1), "tp")
    normed = rows_f * lax.rsqrt(squares[:, None] / D + EPSILON)
    normed = (normed * expert_norm_gain.astype(jnp.float32)[None, :]).astype(jnp.bfloat16)
    packed = jnp.dot(chooser, normed, preferred_element_type=jnp.float32).astype(jnp.bfloat16)
    packed = packed.reshape(bucket_shape + (normed.shape[1],))
    row_block = lax.all_gather(
        lax.all_to_all(packed, "sp", split_axis=0, concat_axis=0, tiled=True),
        "tp",
        axis=3,
        tiled=True,
    )
    served = expert_work(row_block, gate_weight, up_weight, down_weight)
    returned = lax.all_to_all(served, "sp", split_axis=0, concat_axis=0, tiled=True).reshape(
        -1, served.shape[3]
    )
    mixed = resid.astype(jnp.float32)
    for ordinal in range(TOPK):
        selector = (slot_of[:, ordinal][:, None] == slot_index[None, :]).astype(jnp.bfloat16)
        picked = jnp.dot(selector, returned, preferred_element_type=jnp.float32)
        mixed = mixed + routing_weight[:, ordinal : ordinal + 1] * picked
    return mixed.astype(jnp.bfloat16)


def solution(mesh):
    placed = (
        P("sp", "tp"),
        P("sp", "tp"),
        P("sp", "tp"),
        P("sp", "tp"),
        P("sp", "tp"),
        P("sp", "tp"),
        P("sp", "tp"),
        P("sp"),
        P("tp"),
        P("sp", "tp"),
        P(None, "tp"),
        P("tp"),
        P("sp", None),
        P("sp", None),
        P("sp", None, "tp"),
        P("sp", None, "tp"),
        P("sp", None, "tp"),
    )
    return jax.shard_map(
        per_device, mesh=mesh, in_specs=placed, out_specs=P("sp", "tp"), check_vma=False
    )
```

profile of v0, /device:TPU:0, one launch (start us, length us, event | category | flops | bytes accessed | tf_op | source)
XLA Modules:
  0.0 303.4 jit_solution(6847889655338509931)
XLA Ops:
  6.6 0.8 fusion.74
  7.7 1.5 fusion.81
  9.2 1.3 dynamic-slice
  10.5 2.0 slice_dynamic-update-slice_fusion
  12.5 1.3 broadcast_compare_fusion.1
  13.8 0.7 fusion.78
  15.7 0.9 select_reduce_fusion
  16.7 0.8 select_multiply_fusion
  17.4 1.0 copy.177
  18.5 1.0 copy.183
  19.5 1.1 fusion.61
  20.7 0.7 dynamic-update-slice.1
  21.4 1.4 slice_dynamic-update-slice_fusion.1
  22.8 10.6 %all-reduce.3 = (s32[8]{0:T(128)S(1)}, s32[8]{0:T(128)S(1)}, s32[8]{0:T(128)S(1)}) all-reduce(s32[8]{0:T(128)S(1)} %slice_dynamic-update-slice_fusion.1, s32[8]{0:T(128)S(1)} %dynamic-update-slice.1, s32[8]{0:T(128)S(1)} %get-tuple-element.244), channel_id=1, replica_groups=mesh['sp'=8,'tp'=4] {'sp'}, use_global_device_ids=true, to_apply=%add | all-reduce | flops 24 | bytes 192
  33.4 0.8 copy.162
  34.7 1.0 copy.176
  35.7 1.0 add_divide_fusion
  38.0 9.5 %all-gather.2 = f32[8,1,4]{2,1,0:T(1,128)S(1)} all-gather(f32[1,1,4]{2,1,0:T(1,128)S(1)} %bitcast.270), channel_id=1, replica_groups=mesh['sp'=8,'tp'=4] {'sp'}, dimensions={0}, use_global_device_ids=true | all-gather | bytes 144 | tf_op jit(solution)/shard_map/all_gather | solution.py:16
  47.5 10.1 %all-gather.1 = f32[8,1,4]{2,1,0:T(1,128)S(1)} all-gather(f32[1,1,4]{2,1,0:T(1,128)S(1)} %get-tuple-element.235), channel_id=1, replica_groups=mesh['sp'=8,'tp'=4] {'sp'}, dimensions={0}, use_global_device_ids=true | all-gather | bytes 144 | tf_op jit(solution)/shard_map/all_gather | solution.py:16
  57.7 12.8 %all_gather.53 = f32[8,4,128]{2,1,0:T(4,128)S(1)} all-gather(f32[1,4,128]{2,1,0:T(4,128)S(1)} %bitcast.267), channel_id=1, replica_groups=mesh['sp'=8,'tp'=4] {'sp'}, dimensions={0}, use_global_device_ids=true | all-gather | bytes 18432 | tf_op jit(solution)/shard_map/all_gather | solution.py:16
  73.1 9.6 %all_gather.54 = bf16[128,2048]{0,1:T(8,128)(2,1)S(1)} all-gather(bf16[128,512]{0,1:T(8,128)(2,1)S(1)} %bitcast.254), channel_id=1, replica_groups=mesh['sp'=8,'tp'=4] {'tp'}, dimensions={1}, use_global_device_ids=true | all-gather | bytes 655360 | tf_op jit(solution)/shard_map/all_gather | solution.py:191
  82.7 3.0 multiply_reduce_fusion
  85.8 9.0 %psum.7 = f32[128]{0:T(128)S(1)} all-reduce(f32[128]{0:T(128)S(1)} %get-tuple-element.252), channel_id=1, replica_groups=mesh['sp'=8,'tp'=4] {'tp'}, use_global_device_ids=true, to_apply=%region_17.18 | all-reduce | flops 128 | bytes 1024 | tf_op jit(solution)/shard_map/psum | solution.py:209
  95.3 67.8 %all_to_all.10 = bf16[8,1,64,1024]{3,2,1,0:T(8,128)(2,1)} all-to-all(bf16[8,1,64,1024]{3,2,1,0:T(8,128)(2,1)S(1)} %bitcast.247), channel_id=1, replica_groups=mesh['sp'=8,'tp'=4] {'sp'}, dimensions={0} | all-to-all | bytes 2097152 | tf_op jit(solution)/shard_map/all_to_all | solution.py:215
  163.1 50.6 %all-gather.7.cloned.1.call-done = bf16[8,1,64,4096]{3,2,0,1:T(8,128)(2,1)} async-done(((bf16[8,1,64,1024]{3,2,0,1:T(8,128)(2,1)}), bf16[8,1,64,4096]{3,2,0,1:T(8,128)(2,1)}) %all-gather.7.cloned.1.call-update) | async-done | bytes 4194320 | tf_op jit(solution)/shard_map/all_gather | solution.py:214
  213.7 5.9 %fusion.26 = f32[8,1,64,512]{3,2,0,1:T(8,128)S(1)} fusion(bf16[1,4096,512]{2,1,0:T(8,128)(2,1)} %param.33, bf16[8,1,64,4096]{3,2,0,1:T(8,128)(2,1)} %all-gather.7.cloned.1.call-done), kind=kOutput, calls=%fused_computation.33 | convolution fusion | flops 2147483648 | bytes 9437184 | tf_op jit(solution)/shard_map/sqid,qdf->sqif/dot_general | solution.py:141
  219.7 3.2 %fusion.41 = bf16[8,1,64,512]{3,2,0,1:T(8,128)(2,1)} fusion(bf16[1,4096,512]{2,1,0:T(8,128)(2,1)S(1)} %copy-done.8, bf16[8,1,64,4096]{3,2,0,1:T(8,128)(2,1)S(1)} %copy-done.9, f32[8,1,64,512]{3,2,0,1:T(8,128)S(1)} %fusion.26), kind=kOutput, calls=%fused_computation.36 | convolution fusion | flops 2149056512 | bytes 9961472 | tf_op jit(solution)/shard_map/sqid,qdf->sqif/dot_general | solution.py:144
  222.9 35.2 %all-gather.9.cloned.1.call-done = bf16[8,1,64,2048]{3,2,0,1:T(8,128)(2,1)} async-done(((bf16[8,1,64,512]{3,2,0,1:T(8,128)(2,1)}), bf16[8,1,64,2048]{3,2,0,1:T(8,128)(2,1)}) %all-gather.9.cloned.1.call-update) | async-done | bytes 2097168 | tf_op jit(solution)/shard_map/all_gather | solution.py:148
  258.1 6.1 %fusion.21 = bf16[8,1,64,1024]{3,2,1,0:T(8,128)(2,1)} fusion(bf16[1,2048,1024]{2,1,0:T(8,128)(2,1)} %param.35, bf16[8,1,64,2048]{3,2,0,1:T(8,128)(2,1)} %all-gather.9.cloned.1.call-done), kind=kOutput, calls=%fused_computation.32 | convolution fusion | flops 2148007936 | bytes 7340032 | tf_op jit(solution)/shard_map/sqif,qfe->sqie/dot_general | solution.py:146
  264.3 4.6 %all-to-all-start.1 = ((bf16[8,1,64,1024]{3,2,1,0:T(8,128)(2,1)}), bf16[8,1,64,1024]{3,2,1,0:T(8,128)(2,1)S(1)}, u32[]{:S(2)}, u32[]{:S(2)}) async-start(bf16[8,1,64,1024]{3,2,1,0:T(8,128)(2,1)} %fusion.21), calls=%async_computation.1 | async-start | bytes 2097152 | tf_op jit(solution)/shard_map/all_to_all | solution.py:221
  268.9 26.5 %all-to-all-done.1 = bf16[8,1,64,1024]{3,2,1,0:T(8,128)(2,1)S(1)} async-done(((bf16[8,1,64,1024]{3,2,1,0:T(8,128)(2,1)}), bf16[8,1,64,1024]{3,2,1,0:T(8,128)(2,1)S(1)}, u32[]{:S(2)}, u32[]{:S(2)}) %all-to-all-start.1) | async-done | bytes 1048608 | tf_op jit(solution)/shard_map/all_to_all | solution.py:221
  295.8 1.1 fusion.48
  (77 shorter events, 6.3 us)
Async XLA Ops:
  6.5 64.0 %copy-start.2 = (s32[128]{0:T(128)S(1)}, s32[128]{0:T(128)}, u32[]{:S(2)}) copy-start(s32[128]{0:T(128)} %param.26) | copy-start | bytes 1540
  6.5 64.1 %copy-start.3 = (f32[128,4]{0,1:T(4,128)S(1)}, f32[128,4]{0,1:T(4,128)}, u32[]{:S(2)}) copy-start(f32[128,4]{0,1:T(4,128)} %param.23) | copy-start | bytes 6148
  6.5 51.1 %copy-start = (bf16[128,512]{1,0:T(8,128)(2,1)S(1)}, bf16[128,512]{1,0:T(8,128)(2,1)}, u32[]{:S(2)}) copy-start(bf16[128,512]{1,0:T(8,128)(2,1)} %param.20) | copy-start | bytes 393220
  6.5 63.9 %copy-start.4 = (s32[128,2]{0,1:T(2,128)S(1)}, s32[128,2]{0,1:T(2,128)}, u32[]{:S(2)}) copy-start(s32[128,2]{0,1:T(2,128)} %param.31) | copy-start | bytes 3076
  6.5 31.4 %copy-start.6 = (bf16[1024]{0:T(1024)(128)(2,1)S(1)}, bf16[1024]{0:T(1024)(128)(2,1)}, u32[]{:S(2)}) copy-start(bf16[1024]{0:T(1024)(128)(2,1)} %param.30) | copy-start | bytes 6148
  6.5 64.3 %all-gather.11.cloned.1.call-start = ((), (), s32[]{:S(2)}) async-start(), calls=%async_computation.4 | async-start | bytes 2359296 | tf_op jit(solution)/shard_map/all_gather | solution.py:16
  20.6 193.2 %all-gather.7.cloned.1.call-start = ((), (), s32[]{:S(2)}) async-start(), calls=%async_computation.2 | async-start | bytes 5242880 | tf_op jit(solution)/shard_map/all_gather | solution.py:214
  57.7 15.3 %copy-start.5 = (f32[512]{0:T(512)S(1)}, f32[512]{0:T(512)}, u32[]{:S(2)}) copy-start(f32[512]{0:T(512)} %param.27) | copy-start | bytes 6148
  70.9 11.8 %copy-start.1 = (bf16[128,1024]{1,0:T(8,128)(2,1)S(1)}, bf16[128,1024]{1,0:T(8,128)(2,1)}, u32[]{:S(2)}) copy-start(bf16[128,1024]{1,0:T(8,128)(2,1)} %param.28) | copy-start | bytes 786436
  163.1 95.1 %all-gather.9.cloned.1.call-start = ((), (), s32[]{:S(2)}) async-start(), calls=%async_computation.3 | async-start | bytes 2621440 | tf_op jit(solution)/shard_map/all_gather | solution.py:148
  213.7 5.9 %copy-start.8 = (bf16[1,4096,512]{2,1,0:T(8,128)(2,1)S(1)}, bf16[1,4096,512]{2,1,0:T(8,128)(2,1)}, u32[]{:S(2)}) copy-start(bf16[1,4096,512]{2,1,0:T(8,128)(2,1)} %param.34) | copy-start | bytes 12582916
  213.7 5.9 %copy-start.9 = (bf16[8,1,64,4096]{3,2,0,1:T(8,128)(2,1)S(1)}, bf16[8,1,64,4096]{3,2,0,1:T(8,128)(2,1)}, u32[]{:S(2)}) copy-start(bf16[8,1,64,4096]{3,2,0,1:T(8,128)(2,1)} %all-gather.7.cloned.1.call-done) | copy-start | bytes 12582916
  222.9 46.0 %copy-start.7 = (f32[128,2]{0,1:T(2,128)S(1)}, f32[128,2]{0,1:T(2,128)}, u32[]{:S(2)}) copy-start(f32[128,2]{0,1:T(2,128)} %param.32) | copy-start | bytes 3076
  264.3 31.2 %all-to-all-start.1 = ((bf16[8,1,64,1024]{3,2,1,0:T(8,128)(2,1)}), bf16[8,1,64,1024]{3,2,1,0:T(8,128)(2,1)S(1)}, u32[]{:S(2)}, u32[]{:S(2)}) async-start(bf16[8,1,64,1024]{3,2,1,0:T(8,128)(2,1)} %fusion.21), calls=%async_computation.1 | async-start | bytes 2097152 | tf_op jit(solution)/shard_map/all_to_all | solution.py:221
Sparse Core Ops, SparseCore 0:
  20.7 31.9 all-gather.10
  163.2 50.5 all-gather.6
  223.1 35.0 all-gather.8
where the time goes:
time: 304 us; the launch traced here: 303 us
  blocking collectives  129 us (42%)
  waiting for transfers between devices  112 us (37%)
  matrix products  22.8 us (8%)
  between operations  14.1 us (5%)
  local copies, waits for them, and re-layouts  10.6 us (3%)
  other arithmetic  9.33 us (3%)
  starting transfers between devices  4.73 us (2%)
    all_to_all x1, blocking collectives, per_device(): lax.all_to_all(packed, 'sp', split_axis=0, concat_axis=0, tiled=True)  67.8 us
    all_gather x1, waiting for transfers between devices, per_device(): lax.all_gather(lax.all_to_all(packed, 'sp', split_axis=0, concat_axis=0,...  50.6 us
    all_gather x1, waiting for transfers between devices, expert_work(): lax.all_gather(hidden, 'tp', axis=3, tiled=True)  35.2 us
    all_gather x3, blocking collectives, prefix_2(): gathered = jax.tree.map(lambda a: lax.all_gather(a, axis), part)  32.4 us
    all_to_all x1, waiting for transfers between devices, per_device(): lax.all_to_all(served, 'sp', split_axis=0, concat_axis=0, tiled=True)  26.5 us
    unnamed x1, blocking collectives  10.6 us
    all_gather x1, blocking collectives, per_device(): lax.all_gather(memory_cell_output, 'tp', axis=1, tiled=True)  9.63 us
    psum x1, blocking collectives, per_device(): squares = lax.psum(jnp.sum(rows_f * rows_f, axis=1), 'tp')  8.98 us
  transfers between devices with their start and end apart: 4, of which 3 were waited for; matrix products, arithmetic and copies ran while one was open for 2% of the time, Pallas kernels for 0%

commit v1 on v0

--- a/solution.py
+++ b/solution.py
@@ -143,12 +143,22 @@
     )
     upward = jnp.einsum("sqid,qdf->sqif", row_block, up_weight, preferred_element_type=jnp.float32)
     hidden = (jax.nn.silu(gate_act) * upward).astype(jnp.bfloat16)
-    result = jnp.einsum(
-        "sqif,qfe->sqie",
-        lax.all_gather(hidden, "tp", axis=3, tiled=True),
-        down_weight,
-        preferred_element_type=jnp.float32,
-    )
+    peers, mine, width_2 = (lax.axis_size("tp"), lax.axis_index("tp"), hidden.shape[3])
+    forward = [(i, (i + 1) % peers) for i in range(peers)]
+    held, subtotal = (hidden, None)
+    for turn_2 in range(peers):
+        upcoming = lax.ppermute(held, "tp", forward) if turn_2 < peers - 1 else None
+        take_in = jnp.einsum(
+            "sqif,qfe->sqie",
+            held,
+            lax.dynamic_slice_in_dim(
+                down_weight, (mine - turn_2) % peers * width_2, held.shape[3], axis=1
+            ),
+            preferred_element_type=jnp.float32,
+        )
+        subtotal = take_in if subtotal is None else subtotal + take_in
+        held = upcoming
+    result = subtotal
     return result.astype(jnp.bfloat16)
 
 

time: 304 us -> 303 us (level)
    all_gather x1 -> x0, waiting for transfers between devices: 35.2 us -> none  [expert_work(): lax.all_gather(hidden, 'tp', axis=3, tiled=True)]
    ppermute x0 -> x3, waiting for transfers between devices: none -> 35 us  [expert_work(): upcoming = lax.ppermute(held, 'tp', forward) if turn_2 < peers - 1 else None]
    dot_general x1 -> x4, matrix products: 6.14 us -> 5.29 us  [expert_work(): jnp.einsum('sqif,qfe->sqie', held, lax.dynamic_slice_in_dim(down_weight,...]
    unnamed x28 -> x30, local copies, waits for them, and re-layouts: 6.26 us -> 6.26 us
  transfers between devices with their start and end apart: 4 -> 6, of which waited for: 3 -> 5; matrix products, arithmetic and copies ran while one was open for 2% -> 4% of each run, Pallas kernels for 0% -> 0%
where the time goes in v1:
time: 303 us; the launch traced here: 302 us
  blocking collectives  127 us (42%)
  waiting for transfers between devices  112 us (37%)
  matrix products  21.1 us (7%)
  between operations  14.4 us (5%)
  local copies, waits for them, and re-layouts  10.6 us (3%)
  other arithmetic  9.33 us (3%)
  starting transfers between devices  6.77 us (2%)
    all_to_all x1, blocking collectives, per_device(): lax.all_to_all(packed, 'sp', split_axis=0, concat_axis=0, tiled=True)  65.6 us
    all_gather x1, waiting for transfers between devices, per_device(): lax.all_gather(lax.all_to_all(packed, 'sp', split_axis=0, concat_axis=0,...  50.7 us
    ppermute x3, waiting for transfers between devices, expert_work(): upcoming = lax.ppermute(held, 'tp', forward) if turn_2 < peers - 1 else None  35 us
    all_gather x3, blocking collectives, prefix_2(): gathered = jax.tree.map(lambda a: lax.all_gather(a, axis), part)  32.4 us
    all_to_all x1, waiting for transfers between devices, per_device(): lax.all_to_all(served, 'sp', split_axis=0, concat_axis=0, tiled=True)  26.5 us
    unnamed x1, blocking collectives  10.6 us
    all_gather x1, blocking collectives, per_device(): lax.all_gather(memory_cell_output, 'tp', axis=1, tiled=True)  9.65 us
    psum x1, blocking collectives, per_device(): squares = lax.psum(jnp.sum(rows_f * rows_f, axis=1), 'tp')  8.96 us
  transfers between devices with their start and end apart: 6, of which 5 were waited for; matrix products, arithmetic and copies ran while one was open for 4% of the time, Pallas kernels for 0%

profile of v1, /device:TPU:0, one launch (start us, length us, event | category | flops | bytes accessed | tf_op | source)
XLA Modules:
  0.0 301.8 jit_solution(4216754828797818057)
XLA Ops:
  7.7 1.5 fusion.88
  9.2 1.3 dynamic-slice
  10.5 2.0 slice_dynamic-update-slice_fusion
  12.5 1.3 broadcast_compare_fusion.1
  15.7 0.9 select_reduce_fusion
  17.4 1.0 copy.177
  18.5 1.0 copy.183
  19.5 1.1 fusion.64
  21.4 1.4 slice_dynamic-update-slice_fusion.1
  22.8 10.6 %all-reduce.3 = (s32[8]{0:T(128)S(1)}, s32[8]{0:T(128)S(1)}, s32[8]{0:T(128)S(1)}) all-reduce(s32[8]{0:T(128)S(1)} %slice_dynamic-update-slice_fusion.1, s32[8]{0:T(128)S(1)} %dynamic-update-slice.1, s32[8]{0:T(128)S(1)} %get-tuple-element.244), channel_id=1, replica_groups=mesh['sp'=8,'tp'=4] {'sp'}, use_global_device_ids=true, to_apply=%add | all-reduce | flops 24 | bytes 192
  33.4 0.8 copy.162
  34.7 1.0 copy.176
  35.7 1.0 add_divide_fusion
  38.0 9.5 %all-gather.2 = f32[8,1,4]{2,1,0:T(1,128)S(1)} all-gather(f32[1,1,4]{2,1,0:T(1,128)S(1)} %bitcast.281), channel_id=1, replica_groups=mesh['sp'=8,'tp'=4] {'sp'}, dimensions={0}, use_global_device_ids=true | all-gather | bytes 144 | tf_op jit(solution)/shard_map/all_gather | solution.py:16
  47.5 10.1 %all-gather.1 = f32[8,1,4]{2,1,0:T(1,128)S(1)} all-gather(f32[1,1,4]{2,1,0:T(1,128)S(1)} %get-tuple-element.235), channel_id=1, replica_groups=mesh['sp'=8,'tp'=4] {'sp'}, dimensions={0}, use_global_device_ids=true | all-gather | bytes 144 | tf_op jit(solution)/shard_map/all_gather | solution.py:16
  57.7 12.8 %all_gather.50 = f32[8,4,128]{2,1,0:T(4,128)S(1)} all-gather(f32[1,4,128]{2,1,0:T(4,128)S(1)} %bitcast.278), channel_id=1, replica_groups=mesh['sp'=8,'tp'=4] {'sp'}, dimensions={0}, use_global_device_ids=true | all-gather | bytes 18432 | tf_op jit(solution)/shard_map/all_gather | solution.py:16
  73.1 9.6 %all_gather.51 = bf16[128,2048]{0,1:T(8,128)(2,1)S(1)} all-gather(bf16[128,512]{0,1:T(8,128)(2,1)S(1)} %bitcast.265), channel_id=1, replica_groups=mesh['sp'=8,'tp'=4] {'tp'}, dimensions={1}, use_global_device_ids=true | all-gather | bytes 655360 | tf_op jit(solution)/shard_map/all_gather | solution.py:201
  82.7 3.0 %multiply_reduce_fusion = (f32[128]{0:T(128)S(1)}, f32[128,1024]{1,0:T(8,128)S(1)}) fusion(bf16[128,2048]{0,1:T(8,128)(2,1)S(1)} %all_gather.51, bf16[2048,1024]{1,0:T(8,128)(2,1)} %param.29, bf16[128,1024]{1,0:T(8,128)(2,1)S(1)} %copy-done.1), kind=kOutput, calls=%fused_computation.68 | convolution fusion | flops 537657216 | bytes 5505536 | tf_op jit(solution)/shard_map/dot_general | solution.py:200
  85.8 9.0 %psum.7 = f32[128]{0:T(128)S(1)} all-reduce(f32[128]{0:T(128)S(1)} %get-tuple-element.252), channel_id=1, replica_groups=mesh['sp'=8,'tp'=4] {'tp'}, use_global_device_ids=true, to_apply=%region_17.18 | all-reduce | flops 128 | bytes 1024 | tf_op jit(solution)/shard_map/psum | solution.py:219
  95.3 65.6 %all_to_all.10 = bf16[8,1,64,1024]{3,2,1,0:T(8,128)(2,1)} all-to-all(bf16[8,1,64,1024]{3,2,1,0:T(8,128)(2,1)S(1)} %bitcast.258), channel_id=1, replica_groups=mesh['sp'=8,'tp'=4] {'sp'}, dimensions={0} | all-to-all | bytes 2097152 | tf_op jit(solution)/shard_map/all_to_all | solution.py:225
  160.9 50.7 %all-gather.6.cloned.1.call-done = bf16[8,1,64,4096]{3,2,0,1:T(8,128)(2,1)} async-done(((bf16[8,1,64,1024]{3,2,0,1:T(8,128)(2,1)}), bf16[8,1,64,4096]{3,2,0,1:T(8,128)(2,1)}) %all-gather.6.cloned.1.call-update) | async-done | bytes 4194320 | tf_op jit(solution)/shard_map/all_gather | solution.py:224
  211.5 5.9 %fusion.14 = f32[8,1,64,512]{3,2,0,1:T(8,128)S(1)} fusion(bf16[1,4096,512]{2,1,0:T(8,128)(2,1)} %param.33, bf16[8,1,64,4096]{3,2,0,1:T(8,128)(2,1)} %all-gather.6.cloned.1.call-done), kind=kOutput, calls=%fused_computation.30 | convolution fusion | flops 2147483648 | bytes 9437184 | tf_op jit(solution)/shard_map/sqid,qdf->sqif/dot_general | solution.py:141
  217.5 2.4 fusion.29
  219.9 1.5 collective-permute-start
  221.4 12.9 %collective-permute-done = bf16[8,1,64,512]{3,2,0,1:T(8,128)(2,1)S(1)} collective-permute-done((bf16[8,1,64,512]{3,2,0,1:T(8,128)(2,1)S(1)}, bf16[8,1,64,512]{3,2,0,1:T(8,128)(2,1)S(1)}, u32[]{:S(2)}, u32[]{:S(2)}) %collective-permute-start) | collective-permute-done | bytes 524320 | tf_op jit(solution)/shard_map/ppermute | solution.py:150
  234.9 2.1 fusion.50
  237.0 10.9 %collective-permute-done.1 = bf16[8,1,64,512]{3,2,0,1:T(8,128)(2,1)S(1)} collective-permute-done((bf16[8,1,64,512]{3,2,0,1:T(8,128)(2,1)S(1)}, bf16[8,1,64,512]{3,2,0,1:T(8,128)(2,1)S(1)}, u32[]{:S(2)}, u32[]{:S(2)}) %collective-permute-start.1) | collective-permute-done | bytes 524320 | tf_op jit(solution)/shard_map/ppermute | solution.py:150
  249.4 11.2 %collective-permute-done.2 = bf16[8,1,64,512]{3,2,0,1:T(8,128)(2,1)S(1)} collective-permute-done((bf16[8,1,64,512]{3,2,0,1:T(8,128)(2,1)S(1)}, bf16[8,1,64,512]{3,2,0,1:T(8,128)(2,1)S(1)}, u32[]{:S(2)}, u32[]{:S(2)}) %collective-permute-start.2) | collective-permute-done | bytes 524320 | tf_op jit(solution)/shard_map/ppermute | solution.py:150
  260.6 1.8 fusion.13
  262.4 4.6 %all-to-all-start.1 = ((bf16[8,1,64,1024]{3,2,1,0:T(8,128)(2,1)}), bf16[8,1,64,1024]{3,2,1,0:T(8,128)(2,1)S(1)}, u32[]{:S(2)}, u32[]{:S(2)}) async-start(bf16[8,1,64,1024]{3,2,1,0:T(8,128)(2,1)} %fusion.13), calls=%async_computation.1 | async-start | bytes 2097152 | tf_op jit(solution)/shard_map/all_to_all | solution.py:231
  267.0 26.5 %all-to-all-done.1 = bf16[8,1,64,1024]{3,2,1,0:T(8,128)(2,1)S(1)} async-done(((bf16[8,1,64,1024]{3,2,1,0:T(8,128)(2,1)}), bf16[8,1,64,1024]{3,2,1,0:T(8,128)(2,1)S(1)}, u32[]{:S(2)}, u32[]{:S(2)}) %all-to-all-start.1) | async-done | bytes 1048608 | tf_op jit(solution)/shard_map/all_to_all | solution.py:231
  293.9 1.1 fusion.36
  (85 shorter events, 11.2 us)
Async XLA Ops:
  6.5 64.0 %copy-start.3 = (s32[128]{0:T(128)S(1)}, s32[128]{0:T(128)}, u32[]{:S(2)}) copy-start(s32[128]{0:T(128)} %param.26) | copy-start | bytes 1540
  6.5 64.1 %copy-start.4 = (f32[128,4]{0,1:T(4,128)S(1)}, f32[128,4]{0,1:T(4,128)}, u32[]{:S(2)}) copy-start(f32[128,4]{0,1:T(4,128)} %param.23) | copy-start | bytes 6148
  6.5 51.1 %copy-start = (bf16[128,512]{1,0:T(8,128)(2,1)S(1)}, bf16[128,512]{1,0:T(8,128)(2,1)}, u32[]{:S(2)}) copy-start(bf16[128,512]{1,0:T(8,128)(2,1)} %param.20) | copy-start | bytes 393220
  6.5 63.9 %copy-start.5 = (s32[128,2]{0,1:T(2,128)S(1)}, s32[128,2]{0,1:T(2,128)}, u32[]{:S(2)}) copy-start(s32[128,2]{0,1:T(2,128)} %param.31) | copy-start | bytes 3076
  6.5 31.4 %copy-start.7 = (bf16[1024]{0:T(1024)(128)(2,1)S(1)}, bf16[1024]{0:T(1024)(128)(2,1)}, u32[]{:S(2)}) copy-start(bf16[1024]{0:T(1024)(128)(2,1)} %param.30) | copy-start | bytes 6148
  6.5 64.3 %all-gather.8.cloned.1.call-start = ((), (), s32[]{:S(2)}) async-start(), calls=%async_computation.3 | async-start | bytes 2359296 | tf_op jit(solution)/shard_map/all_gather | solution.py:16
  20.6 190.9 %all-gather.6.cloned.1.call-start = ((), (), s32[]{:S(2)}) async-start(), calls=%async_computation.2 | async-start | bytes 5242880 | tf_op jit(solution)/shard_map/all_gather | solution.py:224
  57.7 15.3 %copy-start.6 = (f32[512]{0:T(512)S(1)}, f32[512]{0:T(512)}, u32[]{:S(2)}) copy-start(f32[512]{0:T(512)} %param.27) | copy-start | bytes 6148
  70.9 11.8 %copy-start.1 = (bf16[128,1024]{1,0:T(8,128)(2,1)S(1)}, bf16[128,1024]{1,0:T(8,128)(2,1)}, u32[]{:S(2)}) copy-start(bf16[128,1024]{1,0:T(8,128)(2,1)} %param.28) | copy-start | bytes 786436
  211.5 5.9 %copy-start.9 = (bf16[1,4096,512]{2,1,0:T(8,128)(2,1)S(1)}, bf16[1,4096,512]{2,1,0:T(8,128)(2,1)}, u32[]{:S(2)}) copy-start(bf16[1,4096,512]{2,1,0:T(8,128)(2,1)} %param.34) | copy-start | bytes 12582916
  211.5 5.9 %copy-start.10 = (bf16[8,1,64,4096]{3,2,0,1:T(8,128)(2,1)S(1)}, bf16[8,1,64,4096]{3,2,0,1:T(8,128)(2,1)}, u32[]{:S(2)}) copy-start(bf16[8,1,64,4096]{3,2,0,1:T(8,128)(2,1)} %all-gather.6.cloned.1.call-done) | copy-start | bytes 12582916
  219.9 14.5 %collective-permute-start = (bf16[8,1,64,512]{3,2,0,1:T(8,128)(2,1)S(1)}, bf16[8,1,64,512]{3,2,0,1:T(8,128)(2,1)S(1)}, u32[]{:S(2)}, u32[]{:S(2)}) collective-permute-start(bf16[8,1,64,512]{3,2,0,1:T(8,128)(2,1)S(1)} %fusion.29), channel_id=1, source_target_pairs={{0,1},{1,2},{2,3},{3,0},{4,5},{5,6},{6,7},{7,4},{8,9},{9,10},{10,1... | collective-permute-start | bytes 1572872 | tf_op jit(solution)/shard_map/ppermute | solution.py:150
  234.4 13.5 %collective-permute-start.1 = (bf16[8,1,64,512]{3,2,0,1:T(8,128)(2,1)S(1)}, bf16[8,1,64,512]{3,2,0,1:T(8,128)(2,1)S(1)}, u32[]{:S(2)}, u32[]{:S(2)}) collective-permute-start(bf16[8,1,64,512]{3,2,0,1:T(8,128)(2,1)S(1)} %collective-permute-done), channel_id=1, source_target_pairs={{0,1},{1,2},{2,3},{3,0},{4,5},{5,6},{6,7},{7,4},{8,9},{9,10},{10,1... | collective-permute-start | bytes 1572872 | tf_op jit(solution)/shard_map/ppermute | solution.py:150
  234.9 13.0 %copy-start.2 = (bf16[1,2048,1024]{2,1,0:T(8,128)(2,1)S(1)}, bf16[1,2048,1024]{2,1,0:T(8,128)(2,1)}, u32[]{:S(2)}) copy-start(bf16[1,2048,1024]{2,1,0:T(8,128)(2,1)} %param.35) | copy-start | bytes 12582916
  247.9 12.7 %collective-permute-start.2 = (bf16[8,1,64,512]{3,2,0,1:T(8,128)(2,1)S(1)}, bf16[8,1,64,512]{3,2,0,1:T(8,128)(2,1)S(1)}, u32[]{:S(2)}, u32[]{:S(2)}) collective-permute-start(bf16[8,1,64,512]{3,2,0,1:T(8,128)(2,1)S(1)} %collective-permute-done.1), channel_id=1, source_target_pairs={{0,1},{1,2},{2,3},{3,0},{4,5},{5,6},{6,7},{7,4},{8,9},{9,10},{10,1... | collective-permute-start | bytes 1572872 | tf_op jit(solution)/shard_map/ppermute | solution.py:150
  249.4 17.6 %copy-start.8 = (f32[128,2]{0,1:T(2,128)S(1)}, f32[128,2]{0,1:T(2,128)}, u32[]{:S(2)}) copy-start(f32[128,2]{0,1:T(2,128)} %param.32) | copy-start | bytes 3076
  262.4 31.2 %all-to-all-start.1 = ((bf16[8,1,64,1024]{3,2,1,0:T(8,128)(2,1)}), bf16[8,1,64,1024]{3,2,1,0:T(8,128)(2,1)S(1)}, u32[]{:S(2)}, u32[]{:S(2)}) async-start(bf16[8,1,64,1024]{3,2,1,0:T(8,128)(2,1)} %fusion.13), calls=%async_computation.1 | async-start | bytes 2097152 | tf_op jit(solution)/shard_map/all_to_all | solution.py:231
Sparse Core Ops, SparseCore 0:
  20.7 31.9 all-gather.7
  161.0 50.5 all-gather.5
